TPU v7x, 128 devices: a whole 4x4x4 slice. The times are simulated.
128 devices in a mesh: rep: 2 (over x_hi), fs: 4 (over x_lo, core), tp: 16 (over z, y).
Axes of the slice: x: 4 (x_hi: 2, x_lo: 2; x = x_hi * 2 + x_lo), y: 4, z: 4, core: 2. Of those that a mesh axis runs over, the one named last changes fastest.
Arguments:
- inputs: bfloat16 [4096, 4096], P(('rep', 'fs', 'tp')), may hold values from -6 to 6
- w_gate: bfloat16 [4096, 11008], P('fs', 'tp'), may hold values from -0.09375 to 0.09375
- w_up: bfloat16 [4096, 11008], P('fs', 'tp'), may hold values from -0.09375 to 0.09375
- w_down: bfloat16 [11008, 4096], P('tp', 'fs'), may hold values from -0.0546875 to 0.0546875
- d_out: bfloat16 [4096, 4096], P(('rep', 'fs', 'tp')), may hold values from -24 to 24
Outputs:
- grad_inputs: bfloat16 [4096, 4096], P(('rep', 'fs', 'tp'))
- grad_gate: float32 [4096, 11008], P('fs', 'tp')
- grad_up: float32 [4096, 11008], P('fs', 'tp')
- grad_down: float32 [11008, 4096], P('tp', 'fs')
All inputs are finite; a program needn't handle non-finite values.
Results may differ from a plain program's by a relative error of at most 0.00185.
Values may be sent and summed in bfloat16 or wider, within the bound.
A program may use at most 192 MiB of HBM per device.

v0:
```python
import jax
import jax.numpy as jnp
from jax import lax


def stored(values):
    return lax.optimization_barrier(values.astype(jnp.bfloat16)).astype(jnp.float32)


def reference(inputs, w_gate, w_up, w_down, d_out):
    gate_val = stored(jnp.dot(inputs, w_gate, preferred_element_type=jnp.float32))
    up_val = stored(jnp.dot(inputs, w_up, preferred_element_type=jnp.float32))
    back_val = stored(jnp.dot(d_out, w_down.T, preferred_element_type=jnp.float32))
    sigma = jax.nn.sigmoid(gate_val)
    active = gate_val * sigma
    hidden = (active * up_val).astype(jnp.bfloat16)
    d_gate = (back_val * up_val * sigma * (1.0 + gate_val * (1.0 - sigma))).astype(jnp.bfloat16)
    d_up = (back_val * active).astype(jnp.bfloat16)
    grad_inputs = jnp.dot(d_gate, w_gate.T, preferred_element_type=jnp.float32)
    grad_inputs = grad_inputs + jnp.dot(d_up, w_up.T, preferred_element_type=jnp.float32)
    grad_inputs = grad_inputs.astype(jnp.bfloat16)
    grad_gate = jnp.dot(inputs.T, d_gate, preferred_element_type=jnp.float32)
    grad_up = jnp.dot(inputs.T, d_up, preferred_element_type=jnp.float32)
    grad_down = jnp.dot(hidden.T, d_out, preferred_element_type=jnp.float32)
    return (grad_inputs, grad_gate, grad_up, grad_down)


def solution(mesh):
    return reference
```

profile of v0, /device:TPU:0, one launch (start us, length us, event | category | flops | bytes accessed | tf_op | source)
XLA Modules:
  0.0 767.5 jit_solution(43844783580585515)
XLA Ops:
  7.2 0.0 all-gather.22.cloned.1.call-start
  7.2 0.7 all-gather.22.cloned.1.call-update
  7.9 0.0 all-gather.24.cloned.1.call-start
  7.9 0.7 all-gather.24.cloned.1.call-update
  8.6 0.0 all-gather.18.cloned.1.call-start
  8.7 0.7 all-gather.18.cloned.1.call-update
  9.4 0.0 all-gather.20.cloned.1.call-start
  9.4 0.5 all-gather.20.cloned.1.call-update
  10.0 0.0 all-gather.26.cloned.1.call-start
  10.0 0.5 all-gather.26.cloned.1.call-update
  10.5 0.0 reduce-scatter.4.cloned.1.call-start
  10.6 53.5 %all-gather.22.cloned.1.call-done = bf16[512,4096]{1,0:T(8,128)(2,1)} async-done(((bf16[32,4096]{1,0:T(8,128)(2,1)}), bf16[512,4096]{1,0:T(8,128)(2,1)}) %all-gather.22.cloned.1.call-update) | async-done | bytes 4194320 | tf_op args[0]
  64.1 58.5 %all-gather.24.cloned.1.call-done = bf16[4096,688]{0,1:T(8,128)(2,1)} async-done(((bf16[1024,688]{0,1:T(8,128)(2,1)}), bf16[4096,688]{0,1:T(8,128)(2,1)}) %all-gather.24.cloned.1.call-update) | async-done | bytes 5636112 | tf_op args[2]
  122.7 7.0 convolution_convert_fusion.1
  129.6 48.4 %all-gather.18.cloned.1.call-done = bf16[512,4096]{1,0:T(8,128)(2,1)} async-done(((bf16[32,4096]{1,0:T(8,128)(2,1)}), bf16[512,4096]{1,0:T(8,128)(2,1)}) %all-gather.18.cloned.1.call-update) | async-done | bytes 4194320 | tf_op args[4]
  178.1 58.4 %all-gather.20.cloned.1.call-done = bf16[688,4096]{1,0:T(8,128)(2,1)} async-done(((bf16[688,1024]{1,0:T(8,128)(2,1)}), bf16[688,4096]{1,0:T(8,128)(2,1)}) %all-gather.20.cloned.1.call-update) | async-done | bytes 5636112 | tf_op args[3]
  236.5 7.0 convolution_convert_fusion.2
  243.5 53.8 %all-gather.26.cloned.1.call-done = bf16[4096,688]{0,1:T(8,128)(2,1)} async-done(((bf16[1024,688]{0,1:T(8,128)(2,1)}), bf16[4096,688]{0,1:T(8,128)(2,1)}) %all-gather.26.cloned.1.call-update) | async-done | bytes 5636112 | tf_op args[1]
  297.3 0.0 copy-start
  297.3 7.1 convolution_convert_fusion
  304.4 0.0 copy-done
  304.4 3.9 fusion.15
  308.3 9.0 %convolution_add_fusion = f32[512,4096]{1,0:T(8,128)} fusion(f32[512,4096]{1,0:T(8,128)S(1)} %fusion.15, bf16[4096,688]{0,1:T(8,128)(2,1)} %all-gather.24.cloned.1.call-done, bf16[512,688]{0,1:T(8,128)(2,1)S(1)} %convolution_convert_fusion.2, bf16[512,688]{0,1:T(8,128)(2,1)S(1)} %convolution_convert_fusion), kind=kOutput, calls=%fused_computation | convolution fusion | flops 2890596352 | bytes 23822336 | tf_op jit(solution)/dot_general | solution.py:20
  317.3 0.0 reduce-scatter.4.cloned.1.call-update
  317.3 0.0 all-reduce.9.cloned.1.call-start
  317.3 0.0 copy-start.2
  317.4 8.3 %fusion.13 = f32[688,4096]{1,0:T(8,128)} fusion(bf16[512,4096]{1,0:T(8,128)(2,1)} %all-gather.22.cloned.1.call-done, bf16[512,688]{0,1:T(8,128)(2,1)S(1)} %convolution_convert_fusion.2, bf16[512,688]{0,1:T(8,128)(2,1)S(1)} %convolution_convert_fusion), kind=kOutput, calls=%fused_computation.24 | convolution fusion | flops 2888499200 | bytes 16875520 | tf_op jit(solution)/dot_general | solution.py:23
  325.7 0.0 copy-done.2
  325.7 0.0 copy-start.1
  325.7 5.9 fusion.9
  331.6 0.0 copy-done.1
  331.6 6.4 fusion.17
  338.1 0.0 copy-start.3
  338.1 0.0 all-reduce.9.cloned.1.call-update
  338.1 0.6 copy-done.3
  338.7 0.6 dynamic-slice.33
  339.3 65.5 %reduce-scatter.4.cloned.1.call-done = f32[32,4096]{1,0:T(8,128)} async-done(((f32[512,4096]{1,0:T(8,128)}), f32[32,4096]{1,0:T(8,128)}) %reduce-scatter.4.cloned.1.call-update) | async-done | bytes 524304
  404.8 1.8 convert_element_type.38
  406.6 342.9 %all-reduce.9.cloned.1.call-done = (f32[688,4096]{1,0:T(8,128)}, f32[688,4096]{1,0:T(8,128)}, f32[688,4096]{1,0:T(8,128)}) async-done(((f32[688,4096]{1,0:T(8,128)}, f32[688,4096]{1,0:T(8,128)}, f32[688,4096]{1,0:T(8,128)}), (f32[688,4096]{1,0:T(8,128)}, f32[688,4096]{1,0:T(8,128)}, f32[688,4096]{1,0:T(8,128)})) %all-reduce.9.cloned.1.call-update) | async-done | bytes 33816592 | tf_op jit(solution)/dot_general | solution.py:22
  749.5 4.3 constant_dynamic-slice_fusion
  753.9 6.7 dynamic-slice_bitcast_fusion
Async XLA Ops:
  7.2 57.0 %all-gather.22.cloned.1.call-start = ((), (), s32[]{:S(2)}) async-start(), calls=%async_computation.3 | async-start | bytes 4456448 | tf_op args[0]
  7.9 114.8 %all-gather.24.cloned.1.call-start = ((), (), s32[]{:S(2)}) async-start(), calls=%async_computation.4 | async-start | bytes 7045120 | tf_op args[2]
  8.6 169.4 %all-gather.18.cloned.1.call-start = ((), (), s32[]{:S(2)}) async-start(), calls=%async_computation.1 | async-start | bytes 4456448 | tf_op args[4]
  9.4 227.1 %all-gather.20.cloned.1.call-start = ((), (), s32[]{:S(2)}) async-start(), calls=%async_computation.2 | async-start | bytes 7045120 | tf_op args[3]
  10.0 287.3 %all-gather.26.cloned.1.call-start = ((), (), s32[]{:S(2)}) async-start(), calls=%async_computation.5 | async-start | bytes 7045120 | tf_op args[1]
  10.5 394.3 %reduce-scatter.4.cloned.1.call-start = ((), (), s32[]{:S(2)}) async-start(), calls=%async_computation.6 | async-start | bytes 8912896
  297.3 7.1 copy-start
  317.3 432.2 %all-reduce.9.cloned.1.call-start = ((), (), s32[]{:S(2)}) async-start(), calls=%async_computation.7 | async-start | bytes 67633152 | tf_op jit(solution)/dot_general | solution.py:22
  317.3 8.3 %copy-start.2 = (bf16[512,4096]{1,0:T(8,128)(2,1)S(1)}, bf16[512,4096]{1,0:T(8,128)(2,1)}, u32[]{:S(2)}) copy-start(bf16[512,4096]{1,0:T(8,128)(2,1)} %all-gather.18.cloned.1.call-done) | copy-start | bytes 12582916
  325.7 6.0 copy-start.1
  338.1 0.7 copy-start.3
Sparse Core Ops, SparseCore 0:
  10.1 53.9 all-gather.21
  65.8 56.8 all-gather.23
  124.8 53.2 all-gather.17
  179.6 56.8 all-gather.19
  238.0 59.2 all-gather.25
  317.4 87.3 reduce-scatter.3
  407.6 341.9 all-reduce.8
where the time goes:
time: 768 us; the launch traced here: 767 us
  waiting for transfers between devices  684 us (89%)
  matrix products  54.7 us (7%)
  between operations  14.2 us (2%)
  local copies, waits for them, and re-layouts  12.3 us (2%)
    dot_general x1, waiting for transfers between devices, reference(): grad_gate = jnp.dot(inputs.T, d_gate, preferred_element_type=jnp.float32)  343 us
    unnamed x13, waiting for transfers between devices  341 us
  transfers between devices with their start and end apart: 7, of which 7 were waited for; matrix products, arithmetic and copies ran while one was open for 5% of the time, Pallas kernels for 0%

commit v1 on v0

v1 whole, which is shorter than its diff:
```python
import jax
import jax.numpy as jnp
from jax import lax
from jax.experimental import pallas as pl
from jax.experimental.pallas import tpu as pltpu
from jax.sharding import PartitionSpec as P

MESH = pl.DeviceIdType.MESH
CUT = 352


def dot_nt(a, b):
    return lax.dot_general(a, b, (((1,), (1,)), ((), ())), preferred_element_type=jnp.float32)


def dot_tn(a, b):
    return lax.dot_general(a, b, (((0,), (0,)), ((), ())), preferred_element_type=jnp.float32)


def kernel(x_ref, d_ref, wg_ref, wu_ref, wd_ref, gi, og, ou, od, xo0, xo1, do0, do1, xp, dp, xs, ds, wv, xv, dv, pre, hv, h1, hp0, hp1, dxv, r1, r2, r3, t1, t2, t3, wr, p0, send, recv, local):
    xo, do = (xo0, xo1), (do0, do1)
    rep, fs, tp = lax.axis_index("rep"), lax.axis_index("fs"), lax.axis_index("tp")
    core = fs % 2
    xc = rep * 2 + fs // 2
    z, y = tp // 4, tp % 4

    def at_x(v):
        return {"rep": v // 2, "fs": (v % 2) * 2 + core}

    xright, xleft, xfar = at_x((xc + 1) % 4), at_x((xc + 3) % 4), {"rep": 1 - rep}
    yright, yleft = {"tp": z * 4 + (y + 1) % 4}, {"tp": z * 4 + (y + 3) % 4}
    zright, zleft = {"tp": ((z + 1) % 4) * 4 + y}, {"tp": ((z + 3) % 4) * 4 + y}
    partner = {"fs": fs + 1 - 2 * core}
    owners = (fs, (fs + 2) % 4, fs + 1 - 2 * core, 3 - fs)
    counts = [0]

    def keep(src, dst):
        copy = pltpu.make_async_copy(src, dst, local.at[counts[0]])
        counts[0] += 1
        copy.start()
        return copy

    started = []

    def put(src, dst, dev):
        n = len(started)
        copy = pltpu.make_async_remote_copy(src_ref=src, dst_ref=dst, send_sem=send.at[n], recv_sem=recv.at[n], device_id=dev, device_id_type=MESH)
        copy.start()
        started.append(copy)
        return copy

    def block(r):
        return pl.ds(1024 * r, 1024)

    ready = []
    for q, owner in enumerate(owners):
        span = pl.ds(pl.multiple_of(owner * 1024, 1024), 1024)
        ready += [keep(x_ref.at[:, span], xs.at[:, block(q)]), keep(d_ref.at[:, span], ds.at[:, block(q)])]
    for m, ref in enumerate((wg_ref, wu_ref, wd_ref)):
        ready.append(keep(ref, wv.at[m, :, block(0)]))

    barrier = pltpu.get_barrier_semaphore()
    for dev in (xright, xleft, xfar, yright, yleft, zright, zleft, partner):
        pl.semaphore_signal(barrier, inc=1, device_id=dev, device_id_type=MESH)
    pl.semaphore_wait(barrier, 8)
    for copy in ready:
        copy.wait()

    head, tail = pl.ds(0, CUT), pl.ds(CUT, 688 - CUT)
    lo, hi = pl.ds(0, 16), pl.ds(16, 16)
    first, second = pl.ds(0, 2), pl.ds(2, 2)
    gathered = []

    def first_axis(k, xsrc, dsrc):
        return [
            put(xsrc, xo[k].at[0, 1], yright),
            put(dsrc, do[k].at[1, 0], zright),
            put(xsrc, xo[k].at[0, 2], yleft),
            put(dsrc, do[k].at[2, 0], zleft),
        ]

    def first_axis_far(k, c):
        c[0].wait_recv()
        a = put(xo[k].at[0, 1, lo], xo[k].at[0, 3, lo], yright)
        c[1].wait_recv()
        b = put(do[k].at[1, 0, lo], do[k].at[3, 0, lo], zright)
        c[2].wait_recv()
        e = put(xo[k].at[0, 2, hi], xo[k].at[0, 3, hi], yleft)
        c[3].wait_recv()
        f = put(do[k].at[2, 0, hi], do[k].at[3, 0, hi], zleft)
        return [a, e, b, f]

    def hand_x(k, a):
        gathered.append(put(xo[k].at[a, :, :, pl.ds(2048, 2048)], xp.at[k, a], partner))

    def hand_d(k, a):
        gathered.append(put(do[k].at[:, a, :, pl.ds(2048, 2048)], dp.at[k, :, a], partner))

    def second_axis(k, c):
        c[0].wait_recv()
        c[1].wait_recv()
        a = put(xo[k].at[0], xo[k].at[1], zright)
        b = put(xo[k].at[0], xo[k].at[2], zleft)
        c[2].wait_recv()
        c[3].wait_recv()
        e = put(do[k].at[:, 0], do[k].at[:, 1], yright)
        f = put(do[k].at[:, 0], do[k].at[:, 2], yleft)
        hand_x(k, 0)
        hand_d(k, 0)
        return [a, e, b, f]

    def second_axis_far(k, c):
        c[0].wait_recv()
        a = put(xo[k].at[1, first], xo[k].at[3, first], zright)
        hand_x(k, 1)
        c[1].wait_recv()
        b = put(do[k].at[first, 1], do[k].at[first, 3], yright)
        hand_d(k, 1)
        c[2].wait_recv()
        e = put(xo[k].at[2, second], xo[k].at[3, second], zleft)
        hand_x(k, 2)
        c[3].wait_recv()
        f = put(do[k].at[second, 2], do[k].at[second, 3], yleft)
        hand_d(k, 2)
        return [a, e, b, f]

    def finish(k, c):
        c[0].wait_recv()
        c[1].wait_recv()
        hand_x(k, 3)
        c[2].wait_recv()
        c[3].wait_recv()
        hand_d(k, 3)

    far = [put(xs, xo[1].at[0, 0], xfar), put(ds, do[1].at[0, 0], xfar)]
    own1 = first_axis(0, xs, ds)
    w2 = [
        put(wv.at[0, :, block(0)], wv.at[0, :, block(1)], xright),
        put(wv.at[2, :, block(0)], wv.at[2, :, block(1)], xleft),
        put(wv.at[1, head, block(0)], wv.at[1, head, block(1)], xright),
        put(wv.at[1, tail, block(0)], wv.at[1, tail, block(1)], xleft),
    ]
    w1 = [put(wv.at[m, :, block(0)], wv.at[m, :, block(2)], partner) for m in range(3)]
    own0 = [keep(xs, xo[0].at[0, 0]), keep(ds, do[0].at[0, 0])]

    own2 = first_axis_far(0, own1)
    far[0].wait_recv()
    far[1].wait_recv()
    far1 = first_axis(1, xo[1].at[0, 0], do[1].at[0, 0])
    for copy in own0:
        copy.wait()
    own3 = second_axis(0, own2)
    far2 = first_axis_far(1, far1)
    w2[0].wait_recv()
    w3 = [put(wv.at[0, :, block(1)], wv.at[0, :, block(3)], partner)]
    w2[1].wait_recv()
    w3.append(put(wv.at[2, :, block(1)], wv.at[2, :, block(3)], partner))
    own4 = second_axis_far(0, own3)
    far3 = second_axis(1, far2)
    w2[2].wait_recv()
    w2[3].wait_recv()
    w3.append(put(wv.at[1, :, block(1)], wv.at[1, :, block(3)], partner))
    finish(0, own4)

    whole = [keep(xo0, xv), keep(do0, dv)]
    for copy in w1 + w3:
        copy.wait_recv()
    for copy in whole:
        copy.wait()

    def forward(m, acts, n):
        rows = acts[pl.ds(n * 2, 2)].reshape(256, 4096)
        pre[m, :, pl.ds(pl.multiple_of(n * 256, 256), 256)] = dot_nt(wv[m], rows).astype(jnp.bfloat16)

    def pointwise(h):
        @pl.loop(0, 43)
        def _(n):
            rows = pl.ds(pl.multiple_of(n * 16, 16), 16)
            gate, up, back = [pre[m, rows, :].astype(jnp.float32) for m in range(3)]
            sigma = 1.0 / (1.0 + jnp.exp(-gate))
            active = gate * sigma
            h[0, rows, :] = (back * up * sigma * (1.0 + gate * (1.0 - sigma))).astype(jnp.bfloat16)
            h[1, rows, :] = (back * active).astype(jnp.bfloat16)
            h[2, rows, :] = (active * up).astype(jnp.bfloat16)

    for m, acts in enumerate((xv, xv, dv)):
        @pl.loop(0, 2)
        def _(n):
            forward(m, acts, n)

    pointwise(hv)
    swap0 = put(hv, hp0, partner)
    far4 = second_axis_far(1, far3)
    whole = [keep(xo1.at[first], xv.at[first]), keep(xo1.at[2], xv.at[2]), keep(do1.at[:, pl.ds(0, 3)], dv.at[:, pl.ds(0, 3)])]

    @pl.loop(0, 8)
    def _(n):
        span = pl.ds(pl.multiple_of(n * 512, 512), 512)
        total = dot_tn(hv[0], wv[0, :, span]) + dot_tn(hv[1], wv[1, :, span])
        dxv[:, :, :, span] = total.reshape(4, 4, 32, 512)

    def slab(c, k, h):
        span = pl.ds(2048 * c + 1024 * h, 1024)
        return dxv.at[:, k, :, span] if c == 0 else dxv.at[k, :, :, span]

    def part(c, k, h):
        return r2.at[c, h, k]

    ways = ((yleft, yright), (zleft, zright))

    def send_raw(view, way, c, a1, a3):
        return [
            put(view(c, 3, 0), a1.at[c, 0], way[1]),
            put(view(c, 3, 1), a1.at[c, 1], way[0]),
            put(view(c, 2, 1), a3.at[c, 1], way[1]),
            put(view(c, 1, 0), a3.at[c, 0], way[0]),
        ]

    def send_summed(view, way, c, a1, a2, copies):
        copies[0].wait_recv()
        a1[c, 0] += view(c, 2, 0)[...]
        one = put(a1.at[c, 0], a2.at[c, 0], way[1])
        copies[1].wait_recv()
        a1[c, 1] += view(c, 1, 1)[...]
        return [one, put(a1.at[c, 1], a2.at[c, 1], way[0])]

    sums1 = [send_raw(slab, ways[c], c, r1, r3) for c in range(2)]
    whole[0].wait()
    forward(0, xv, 0)
    forward(1, xv, 0)
    finish(1, far4)
    last_x, last_d = keep(xo1.at[3], xv.at[3]), keep(do1.at[:, 3], dv.at[:, 3])
    whole[1].wait()
    last_x.wait()
    forward(0, xv, 1)
    forward(1, xv, 1)
    for copy in gathered:
        copy.wait_recv()

    def load(k, tokens, theirs, r):
        return [
            keep(source, (xv, dv)[k].at[:, :, :, block(q)])
            for q, source in enumerate((tokens[0].at[:, :, :, block(r)], tokens[1].at[:, :, :, block(r)], theirs.at[0, :, :, :, block(r)], theirs.at[1, :, :, :, block(r)]))
        ]

    loads_x = load(0, xo, xp, 1)
    whole[2].wait()
    last_d.wait()

    @pl.loop(0, 2)
    def _(n):
        forward(2, dv, n)

    loads_d = load(1, do, dp, 1)
    pointwise(h1)
    swaps = [put(h1.at[m], hp1.at[m], partner) for m in range(3)]
    sums2 = [send_summed(slab, ways[c], c, r1, r2, sums1[c]) for c in range(2)]

    def product(m, acts, n):
        total = None
        for q, h in enumerate((hv, h1, hp0, hp1)):
            span = pl.ds(pl.multiple_of(q * 1024 + n * 256, 256), 256)
            term = jnp.dot(h[m], acts[:, :, :, span].reshape(512, 256), preferred_element_type=jnp.float32)
            total = term if total is None else total + term
        return total

    crossing = []

    def outgoing(m, acts):
        for half in range(2):
            @pl.loop(2 * half, 2 * half + 2)
            def _(n):
                wv[m, :, pl.ds(pl.multiple_of(n * 256, 256), 256)] = product(m, acts, n).astype(jnp.bfloat16)

            span = pl.ds(512 * half, 512)
            crossing.append(put(wv.at[m, head, span], wr.at[m, head, span], xright))
            crossing.append(put(wv.at[m, tail, span], wr.at[m, tail, span], xleft))

    def kept(m, acts, slot):
        @pl.loop(0, 4)
        def _(n):
            p0[slot, :, pl.ds(pl.multiple_of(n * 256, 256), 256)] = product(m, acts, n)

    def close(m, slot, ref):
        for copy in crossing[4 * m:4 * m + 4]:
            copy.wait_recv()

        @pl.loop(0, 4)
        def _(n):
            span = pl.ds(pl.multiple_of(n * 256, 256), 256)
            p0[slot, :, span] += wr[m, :, span].astype(jnp.float32)

        return keep(p0.at[slot], ref)

    for copy in loads_x:
        copy.wait()
    swap0.wait_recv()
    swaps[0].wait_recv()
    for copy in w1 + w2:
        copy.wait_send()
    outgoing(0, xv)
    swaps[1].wait_recv()
    outgoing(1, xv)
    loads_x = load(0, xo, xp, 0)
    for copy in loads_d:
        copy.wait()
    swaps[2].wait_recv()
    outgoing(2, dv)
    loads_d = load(1, do, dp, 0)
    sums3 = []
    for c in range(2):
        sums1[c][3].wait_recv()
        sums2[c][0].wait_recv()
        r2[c, 0] += slab(c, 0, 0)[...] + r3[c, 0]
        sums1[c][2].wait_recv()
        sums2[c][1].wait_recv()
        r2[c, 1] += slab(c, 0, 1)[...] + r3[c, 1]
        sums3.append(send_raw(part, ways[1 - c], c, t1, t3))
    for copy in loads_x:
        copy.wait()
    kept(0, xv, 0)
    kept(1, xv, 1)
    sums4 = [send_summed(part, ways[1 - c], c, t1, t2, sums3[c]) for c in range(2)]
    out0 = close(0, 0, og)
    for c in range(2):
        sums3[c][3].wait_recv()
        sums4[c][0].wait_recv()
        sums3[c][2].wait_recv()
        sums4[c][1].wait_recv()
        for h in range(2):
            total = part(c, 0, h)[...] + (t2[c, h] + t3[c, h])
            gi[:, pl.ds(pl.multiple_of(owners[2 * c + h] * 1024, 1024), 1024)] = total.astype(jnp.bfloat16)
    for copy in loads_d:
        copy.wait()
    out0.wait()
    kept(2, dv, 0)
    out1 = close(1, 1, ou)
    out2 = close(2, 0, od)
    out1.wait()
    out2.wait()
    for copy in started:
        if not any(copy is done for done in w1 + w2):
            copy.wait_send()


SENDS, KEPT = 100, 39


def body(inputs, w_gate, w_up, w_down, d_out):
    b, f = jnp.bfloat16, jnp.float32
    vm = pl.BlockSpec(memory_space=pltpu.VMEM)
    anys = pl.BlockSpec(memory_space=pl.ANY)
    s = jax.ShapeDtypeStruct
    outs = pl.pallas_call(
        kernel,
        out_shape=[s((32, 4096), b)] + [s((688, 1024), f)] * 3 + [s((4, 4, 32, 4096), b)] * 4 + [s((2, 4, 4, 32, 2048), b)] * 2,
        in_specs=[anys] * 5,
        out_specs=[vm] + [anys] * 9,
        scratch_shapes=[pltpu.VMEM((32, 4096), b)] * 2
        + [pltpu.VMEM((3, 688, 4096), b)]
        + [pltpu.VMEM((4, 4, 32, 4096), b)] * 2
        + [pltpu.VMEM((3, 688, 512), b)] * 5
        + [pltpu.VMEM((4, 4, 32, 4096), f)]
        + [pltpu.VMEM((2, 2, 4, 32, 1024), f)] * 3
        + [pltpu.VMEM((2, 2, 32, 1024), f)] * 3
        + [pltpu.VMEM((3, 688, 1024), b)]
        + [pltpu.VMEM((2, 688, 1024), f)]
        + [pltpu.SemaphoreType.DMA((SENDS,)), pltpu.SemaphoreType.DMA((SENDS,)), pltpu.SemaphoreType.DMA((KEPT,))],
        compiler_params=pltpu.CompilerParams(collective_id=0, has_side_effects=True, vmem_limit_bytes=67043328),
    )(inputs, d_out, w_gate.T, w_up.T, w_down)
    return outs[0], outs[1].T, outs[2].T, outs[3]


def solution(mesh):
    tok = P(("rep", "fs", "tp"), None)
    return jax.shard_map(
        body,
        mesh=mesh,
        in_specs=(tok, P("fs", "tp"), P("fs", "tp"), P("tp", "fs"), tok),
        out_specs=(tok, P("fs", "tp"), P("fs", "tp"), P("tp", "fs")),
        check_vma=False,
    )
```

time: 768 us -> 180 us (0.23)
  waiting for transfers between devices: 684 us -> 0 us
  Pallas kernels: 0 us -> 169 us
  matrix products: 54.7 us -> 0 us
  between operations: 14.2 us -> 0.64 us
    dot_general x1 -> x0, waiting for transfers between devices: 343 us -> none  [reference(): grad_gate = jnp.dot(inputs.T, d_gate, preferred_element_type=jnp.float32)]
    unnamed x13 -> x0, waiting for transfers between devices: 341 us -> none
    pallas_call x0 -> x1, Pallas kernels: none -> 169 us  [body(): pl.pallas_call(kernel, out_shape=[s((32, 4096), b)] + [s((688, 1024), f)]...]
    dot_general x8 -> x0, matrix products: 54.7 us -> none  [the longest x1 8.97 us: reference(): jnp.dot(d_up, w_up.T, preferred_element_type=jnp.float32)]
    dot_general x3 -> x0, local copies, waits for them, and re-layouts: 11.7 us -> none  [the longest x1 6.73 us: reference(): grad_up = jnp.dot(inputs.T, d_up, preferred_element_type=jnp.float32)]
    unnamed x8, local copies, waits for them, and re-layouts: 0.64 us -> 9.9 us
  transfers between devices with their start and end apart: 7 -> 0, of which waited for: 7 -> 0; matrix products, arithmetic and copies ran while one was open for 5% -> 0% of each run, Pallas kernels for 0% -> 0%
where the time goes in v1:
time: 180 us
  Pallas kernels  169 us (94%)
  local copies, waits for them, and re-layouts  9.9 us (6%)
    pallas_call x1, Pallas kernels, body(): pl.pallas_call(kernel, out_shape=[s((32, 4096), b)] + [s((688, 1024), f)]...  169 us
    unnamed x8, local copies, waits for them, and re-layouts  9.9 us

profile of v1, /device:TPU:0, one launch (start us, length us, event | category | flops | bytes accessed | tf_op | source)
XLA Modules:
  0.0 179.7 jit_solution(36553674514738342)
XLA Ops:
  0.6 169.2 %shard_map.84 = (bf16[32,4096]{1,0:T(8,128)(2,1)}, f32[688,1024]{1,0:T(8,128)}, f32[688,1024]{1,0:T(8,128)}, f32[688,1024]{1,0:T(8,128)}, bf16[4,4,32,4096]{3,2,...) custom-call(bf16[32,4096]{1,0:T(8,128)(2,1)} %x_ref.1, ...), custom_call_target="tpu_custom_call" | custom-call | tf_op jit(solution)/shard_map/pallas_call | solution.py:354
  169.8 1.7 copy.13
  171.5 0.0 copy-start.1
  171.5 3.9 %copy.14 = f32[1024,688]{0,1:T(8,128)} copy(f32[1024,688]{0,1:T(8,128)} %bitcast.5) | data formatting | bytes 5636096
  175.4 0.0 copy-done.1
  175.4 0.0 copy-start
  175.4 1.6 copy.15
  176.9 1.3 copy-done
  178.2 1.6 copy.16
Async XLA Ops:
  171.5 3.9 %copy-start.1 = (f32[688,1024]{1,0:T(8,128)S(1)}, f32[688,1024]{1,0:T(8,128)}, u32[]{:S(2)}) copy-start(f32[688,1024]{1,0:T(8,128)} %get-tuple-element.10) | copy-start | bytes 8454148
  175.4 2.8 %copy-start = (f32[688,1024]{1,0:T(8,128)S(1)}, f32[688,1024]{1,0:T(8,128)}, u32[]{:S(2)}) copy-start(f32[688,1024]{1,0:T(8,128)} %get-tuple-element.19) | copy-start | bytes 8454148

commit v2 on v1

--- a/solution.py
+++ b/solution.py
@@ -17,7 +17,7 @@
     return lax.dot_general(a, b, (((0,), (0,)), ((), ())), preferred_element_type=jnp.float32)
 
 
-def kernel(x_ref, d_ref, wg_ref, wu_ref, wd_ref, gi, og, ou, od, xo0, xo1, do0, do1, xp, dp, xs, ds, wv, xv, dv, pre, hv, h1, hp0, hp1, dxv, r1, r2, r3, t1, t2, t3, wr, p0, send, recv, local):
+def kernel(x_ref, d_ref, wg_ref, wu_ref, wd_ref, gi, og, ou, od, xo0, xo1, do0, do1, xp, dp, rx, rd, xs, ds, fx, fd, wv, xv, dv, back_ref, hv, h1, hp0, hp1, dxv, r1, r2, r3, t1, t2, t3, wr, send, recv, local):
     xo, do = (xo0, xo1), (do0, do1)
     rep, fs, tp = lax.axis_index("rep"), lax.axis_index("fs"), lax.axis_index("tp")
     core = fs % 2
@@ -63,7 +63,7 @@
     for dev in (xright, xleft, xfar, yright, yleft, zright, zleft, partner):
         pl.semaphore_signal(barrier, inc=1, device_id=dev, device_id_type=MESH)
     pl.semaphore_wait(barrier, 8)
-    for copy in ready:
+    for copy in ready[:8]:
         copy.wait()
 
     head, tail = pl.ds(0, CUT), pl.ds(CUT, 688 - CUT)
@@ -99,30 +99,34 @@
     def second_axis(k, c):
         c[0].wait_recv()
         c[1].wait_recv()
-        a = put(xo[k].at[0], xo[k].at[1], zright)
-        b = put(xo[k].at[0], xo[k].at[2], zleft)
+        x = [put(xo[k].at[0, half], xo[k].at[slot, half], dev) for half, slot, dev in ((first, 1, zright), (second, 2, zleft), (second, 1, zright), (first, 2, zleft))]
         c[2].wait_recv()
         c[3].wait_recv()
-        e = put(do[k].at[:, 0], do[k].at[:, 1], yright)
-        f = put(do[k].at[:, 0], do[k].at[:, 2], yleft)
+        d = [put(do[k].at[half, 0], do[k].at[half, slot], dev) for half, slot, dev in ((first, 1, yright), (second, 2, yleft), (second, 1, yright), (first, 2, yleft))]
         hand_x(k, 0)
         hand_d(k, 0)
+        return x, d
+
+    def second_axis_far(k, c):
+        first, second = ((pl.ds(0, 2), pl.ds(2, 2)), (pl.ds(0, 1), pl.ds(3, 1)))[k]
+        x, d = c
+        x[0].wait_recv()
+        a = put(xo[k].at[1, first], xo[k].at[3, first], zright)
+        d[0].wait_recv()
+        b = put(do[k].at[first, 1], do[k].at[first, 3], yright)
+        x[1].wait_recv()
+        e = put(xo[k].at[2, second], xo[k].at[3, second], zleft)
+        d[1].wait_recv()
+        f = put(do[k].at[second, 2], do[k].at[second, 3], yleft)
         return [a, e, b, f]
 
-    def second_axis_far(k, c):
-        c[0].wait_recv()
-        a = put(xo[k].at[1, first], xo[k].at[3, first], zright)
-        hand_x(k, 1)
-        c[1].wait_recv()
-        b = put(do[k].at[first, 1], do[k].at[first, 3], yright)
-        hand_d(k, 1)
-        c[2].wait_recv()
-        e = put(xo[k].at[2, second], xo[k].at[3, second], zleft)
-        hand_x(k, 2)
-        c[3].wait_recv()
-        f = put(do[k].at[second, 2], do[k].at[second, 3], yleft)
-        hand_d(k, 2)
-        return [a, e, b, f]
+    def rest(k, c):
+        x, d = c
+        for n in range(2):
+            x[2 + n].wait_recv()
+            hand_x(k, 1 + n)
+            d[2 + n].wait_recv()
+            hand_d(k, 1 + n)
 
     def finish(k, c):
         c[0].wait_recv()
@@ -132,17 +136,23 @@
         c[3].wait_recv()
         hand_d(k, 3)
 
-    far = [put(xs, xo[1].at[0, 0], xfar), put(ds, do[1].at[0, 0], xfar)]
+    hops = [put(xs, fx, xright), put(ds, fd, xleft)]
     own1 = first_axis(0, xs, ds)
+    own0 = [keep(xs, xo[0].at[0, 0]), keep(ds, do[0].at[0, 0])]
+
+    for copy in ready[8:]:
+        copy.wait()
+    w1 = [put(wv.at[m, :, block(0)], wv.at[m, :, block(2)], partner) for m in range(3)]
+    hops[0].wait_recv()
+    far = [put(fx, xo[1].at[0, 0], xright)]
+    hops[1].wait_recv()
+    far.append(put(fd, do[1].at[0, 0], xleft))
     w2 = [
         put(wv.at[0, :, block(0)], wv.at[0, :, block(1)], xright),
         put(wv.at[2, :, block(0)], wv.at[2, :, block(1)], xleft),
         put(wv.at[1, head, block(0)], wv.at[1, head, block(1)], xright),
         put(wv.at[1, tail, block(0)], wv.at[1, tail, block(1)], xleft),
     ]
-    w1 = [put(wv.at[m, :, block(0)], wv.at[m, :, block(2)], partner) for m in range(3)]
-    own0 = [keep(xs, xo[0].at[0, 0]), keep(ds, do[0].at[0, 0])]
-
     own2 = first_axis_far(0, own1)
     far[0].wait_recv()
     far[1].wait_recv()
@@ -151,16 +161,19 @@
         copy.wait()
     own3 = second_axis(0, own2)
     far2 = first_axis_far(1, far1)
+    own4 = second_axis_far(0, own3)
     w2[0].wait_recv()
     w3 = [put(wv.at[0, :, block(1)], wv.at[0, :, block(3)], partner)]
     w2[1].wait_recv()
     w3.append(put(wv.at[2, :, block(1)], wv.at[2, :, block(3)], partner))
-    own4 = second_axis_far(0, own3)
+    rest(0, own3)
     far3 = second_axis(1, far2)
     w2[2].wait_recv()
     w2[3].wait_recv()
     w3.append(put(wv.at[1, :, block(1)], wv.at[1, :, block(3)], partner))
     finish(0, own4)
+    middle = pl.ds(1, 2)
+    helped = [put(xo0.at[3, middle], rx, xright), put(do0.at[middle, 3], rd, xleft)]
 
     whole = [keep(xo0, xv), keep(do0, dv)]
     for copy in w1 + w3:
@@ -168,29 +181,38 @@
     for copy in whole:
         copy.wait()
 
-    def forward(m, acts, n):
+    def forward(ref, m, acts, n):
         rows = acts[pl.ds(n * 2, 2)].reshape(256, 4096)
-        pre[m, :, pl.ds(pl.multiple_of(n * 256, 256), 256)] = dot_nt(wv[m], rows).astype(jnp.bfloat16)
-
-    def pointwise(h):
+        ref[:, pl.ds(pl.multiple_of(n * 256, 256), 256)] = dot_nt(wv[m], rows).astype(jnp.bfloat16)
+
+    def pointwise(h, inner, outer):
         @pl.loop(0, 43)
         def _(n):
             rows = pl.ds(pl.multiple_of(n * 16, 16), 16)
-            gate, up, back = [pre[m, rows, :].astype(jnp.float32) for m in range(3)]
+            gate = h[0, rows, :].astype(jnp.float32)
+            up = h[1, rows, :].astype(jnp.float32)
             sigma = 1.0 / (1.0 + jnp.exp(-gate))
             active = gate * sigma
-            h[0, rows, :] = (back * up * sigma * (1.0 + gate * (1.0 - sigma))).astype(jnp.bfloat16)
-            h[1, rows, :] = (back * active).astype(jnp.bfloat16)
-            h[2, rows, :] = (active * up).astype(jnp.bfloat16)
+            if inner:
+                h[2, rows, :] = (active * up).astype(jnp.bfloat16)
+            if outer:
+                back = back_ref[rows, :].astype(jnp.float32)
+                h[0, rows, :] = (back * up * sigma * (1.0 + gate * (1.0 - sigma))).astype(jnp.bfloat16)
+                h[1, rows, :] = (back * active).astype(jnp.bfloat16)
 
     for m, acts in enumerate((xv, xv, dv)):
         @pl.loop(0, 2)
         def _(n):
-            forward(m, acts, n)
-
-    pointwise(hv)
+            forward((hv.at[0], hv.at[1], back_ref)[m], m, acts, n)
+
+    helped[0].wait_recv()
+    relay = [put(rx, xo1.at[3, middle], xright)]
+    helped[1].wait_recv()
+    relay.append(put(rd, do1.at[middle, 3], xleft))
+    far4 = second_axis_far(1, far3)
+    pointwise(hv, True, True)
     swap0 = put(hv, hp0, partner)
-    far4 = second_axis_far(1, far3)
+    rest(1, far3)
     whole = [keep(xo1.at[first], xv.at[first]), keep(xo1.at[2], xv.at[2]), keep(do1.at[:, pl.ds(0, 3)], dv.at[:, pl.ds(0, 3)])]
 
     @pl.loop(0, 8)
@@ -226,14 +248,18 @@
 
     sums1 = [send_raw(slab, ways[c], c, r1, r3) for c in range(2)]
     whole[0].wait()
-    forward(0, xv, 0)
-    forward(1, xv, 0)
+    forward(h1.at[0], 0, xv, 0)
+    forward(h1.at[1], 1, xv, 0)
+    for copy in relay:
+        copy.wait_recv()
     finish(1, far4)
     last_x, last_d = keep(xo1.at[3], xv.at[3]), keep(do1.at[:, 3], dv.at[:, 3])
     whole[1].wait()
     last_x.wait()
-    forward(0, xv, 1)
-    forward(1, xv, 1)
+    forward(h1.at[0], 0, xv, 1)
+    forward(h1.at[1], 1, xv, 1)
+    pointwise(h1, True, False)
+    swaps = {2: put(h1.at[2], hp1.at[2], partner)}
     for copy in gathered:
         copy.wait_recv()
 
@@ -249,12 +275,12 @@
 
     @pl.loop(0, 2)
     def _(n):
-        forward(2, dv, n)
+        forward(back_ref, 2, dv, n)
 
     loads_d = load(1, do, dp, 1)
-    pointwise(h1)
-    swaps = [put(h1.at[m], hp1.at[m], partner) for m in range(3)]
-    sums2 = [send_summed(slab, ways[c], c, r1, r2, sums1[c]) for c in range(2)]
+    pointwise(h1, False, True)
+    for m in range(2):
+        swaps[m] = put(h1.at[m], hp1.at[m], partner)
 
     def product(m, acts, n):
         total = None
@@ -264,7 +290,7 @@
             total = term if total is None else total + term
         return total
 
-    crossing = []
+    crossing = {}
 
     def outgoing(m, acts):
         for half in range(2):
@@ -273,40 +299,39 @@
                 wv[m, :, pl.ds(pl.multiple_of(n * 256, 256), 256)] = product(m, acts, n).astype(jnp.bfloat16)
 
             span = pl.ds(512 * half, 512)
-            crossing.append(put(wv.at[m, head, span], wr.at[m, head, span], xright))
-            crossing.append(put(wv.at[m, tail, span], wr.at[m, tail, span], xleft))
-
-    def kept(m, acts, slot):
+            crossing[m, half] = [put(wv.at[m, head, span], wr.at[m, head, span], xright), put(wv.at[m, tail, span], wr.at[m, tail, span], xleft)]
+
+    def kept(m, acts, ref):
         @pl.loop(0, 4)
         def _(n):
-            p0[slot, :, pl.ds(pl.multiple_of(n * 256, 256), 256)] = product(m, acts, n)
-
-    def close(m, slot, ref):
-        for copy in crossing[4 * m:4 * m + 4]:
-            copy.wait_recv()
-
-        @pl.loop(0, 4)
-        def _(n):
-            span = pl.ds(pl.multiple_of(n * 256, 256), 256)
-            p0[slot, :, span] += wr[m, :, span].astype(jnp.float32)
-
-        return keep(p0.at[slot], ref)
-
-    for copy in loads_x:
+            ref[:, pl.ds(pl.multiple_of(n * 256, 256), 256)] = product(m, acts, n)
+
+    def close(m, ref):
+        for half in range(2):
+            for copy in crossing[m, half]:
+                copy.wait_recv()
+
+            @pl.loop(2 * half, 2 * half + 2)
+            def _(n):
+                span = pl.ds(pl.multiple_of(n * 256, 256), 256)
+                ref[:, span] += wr[m, :, span].astype(jnp.float32)
+
+    for copy in loads_d:
         copy.wait()
     swap0.wait_recv()
-    swaps[0].wait_recv()
+    swaps[2].wait_recv()
     for copy in w1 + w2:
         copy.wait_send()
+    outgoing(2, dv)
+    loads_d = load(1, do, dp, 0)
+    sums2 = [send_summed(slab, ways[c], c, r1, r2, sums1[c]) for c in range(2)]
+    for copy in loads_x:
+        copy.wait()
+    swaps[0].wait_recv()
     outgoing(0, xv)
     swaps[1].wait_recv()
     outgoing(1, xv)
     loads_x = load(0, xo, xp, 0)
-    for copy in loads_d:
-        copy.wait()
-    swaps[2].wait_recv()
-    outgoing(2, dv)
-    loads_d = load(1, do, dp, 0)
     sums3 = []
     for c in range(2):
         sums1[c][3].wait_recv()
@@ -316,12 +341,15 @@
         sums2[c][1].wait_recv()
         r2[c, 1] += slab(c, 0, 1)[...] + r3[c, 1]
         sums3.append(send_raw(part, ways[1 - c], c, t1, t3))
+    for copy in loads_d:
+        copy.wait()
+    kept(2, dv, od)
     for copy in loads_x:
         copy.wait()
-    kept(0, xv, 0)
-    kept(1, xv, 1)
+    kept(0, xv, og)
+    kept(1, xv, ou)
     sums4 = [send_summed(part, ways[1 - c], c, t1, t2, sums3[c]) for c in range(2)]
-    out0 = close(0, 0, og)
+    close(2, od)
     for c in range(2):
         sums3[c][3].wait_recv()
         sums4[c][0].wait_recv()
@@ -330,20 +358,14 @@
         for h in range(2):
             total = part(c, 0, h)[...] + (t2[c, h] + t3[c, h])
             gi[:, pl.ds(pl.multiple_of(owners[2 * c + h] * 1024, 1024), 1024)] = total.astype(jnp.bfloat16)
-    for copy in loads_d:
-        copy.wait()
-    out0.wait()
-    kept(2, dv, 0)
-    out1 = close(1, 1, ou)
-    out2 = close(2, 0, od)
-    out1.wait()
-    out2.wait()
+    close(0, og)
+    close(1, ou)
     for copy in started:
         if not any(copy is done for done in w1 + w2):
             copy.wait_send()
 
 
-SENDS, KEPT = 100, 39
+SENDS, KEPT, LIMIT = 120, 42, 58000000
 
 
 def body(inputs, w_gate, w_up, w_down, d_out):
@@ -353,20 +375,20 @@
     s = jax.ShapeDtypeStruct
     outs = pl.pallas_call(
         kernel,
-        out_shape=[s((32, 4096), b)] + [s((688, 1024), f)] * 3 + [s((4, 4, 32, 4096), b)] * 4 + [s((2, 4, 4, 32, 2048), b)] * 2,
+        out_shape=[pltpu.VMEM((32, 4096), b)] + [pltpu.VMEM((688, 1024), f)] * 3 + [s((4, 4, 32, 4096), b)] * 4 + [s((2, 4, 4, 32, 2048), b)] * 2 + [s((2, 32, 4096), b)] * 2,
         in_specs=[anys] * 5,
-        out_specs=[vm] + [anys] * 9,
-        scratch_shapes=[pltpu.VMEM((32, 4096), b)] * 2
+        out_specs=[vm] * 4 + [anys] * 8,
+        scratch_shapes=[pltpu.VMEM((32, 4096), b)] * 4
         + [pltpu.VMEM((3, 688, 4096), b)]
         + [pltpu.VMEM((4, 4, 32, 4096), b)] * 2
-        + [pltpu.VMEM((3, 688, 512), b)] * 5
+        + [pltpu.VMEM((688, 512), b)]
+        + [pltpu.VMEM((3, 688, 512), b)] * 4
         + [pltpu.VMEM((4, 4, 32, 4096), f)]
         + [pltpu.VMEM((2, 2, 4, 32, 1024), f)] * 3
         + [pltpu.VMEM((2, 2, 32, 1024), f)] * 3
         + [pltpu.VMEM((3, 688, 1024), b)]
-        + [pltpu.VMEM((2, 688, 1024), f)]
         + [pltpu.SemaphoreType.DMA((SENDS,)), pltpu.SemaphoreType.DMA((SENDS,)), pltpu.SemaphoreType.DMA((KEPT,))],
-        compiler_params=pltpu.CompilerParams(collective_id=0, has_side_effects=True, vmem_limit_bytes=67043328),
+        compiler_params=pltpu.CompilerParams(collective_id=0, has_side_effects=True, vmem_limit_bytes=LIMIT),
     )(inputs, d_out, w_gate.T, w_up.T, w_down)
     return outs[0], outs[1].T, outs[2].T, outs[3]
 

time: 180 us -> 170 us (0.944)
  Pallas kernels: 169 us -> 164 us
  local copies, waits for them, and re-layouts: 9.9 us -> 5.37 us
    pallas_call x1, Pallas kernels: 169 us -> 164 us  [body(): pl.pallas_call(kernel, out_shape=[pltpu.VMEM((32, 4096), b)] + [pltpu.VME...]
    unnamed x8 -> x4, local copies, waits for them, and re-layouts: 9.9 us -> 5.37 us
where the time goes in v2:
time: 170 us
  Pallas kernels  164 us (96%)
  local copies, waits for them, and re-layouts  5.37 us (3%)
    pallas_call x1, Pallas kernels, body(): pl.pallas_call(kernel, out_shape=[pltpu.VMEM((32, 4096), b)] + [pltpu.VME...  164 us
    unnamed x4, local copies, waits for them, and re-layouts  5.37 us

profile of v2, /device:TPU:0, one launch (start us, length us, event | category | flops | bytes accessed | tf_op | source)
XLA Modules:
  0.0 169.6 jit_solution(10236624053842530156)
XLA Ops:
  0.6 163.6 %shard_map.84 = (bf16[32,4096]{1,0:T(8,128)(2,1)S(1)}, f32[688,1024]{1,0:T(8,128)S(1)}, f32[688,1024]{1,0:T(8,128)S(1)}, f32[688,1024]{1,0:T(8,128)S(1)}, bf16[4...) custom-call(bf16[32,4096]{1,0:T(8,128)(2,1)} %x_ref.1, ...), custom_call_target="tpu_custom_call" | custom-call | tf_op jit(solution)/shard_map/pallas_call | solution.py:376
  164.3 0.7 copy.13
  165.0 1.6 copy.14
  166.5 1.6 copy.15
  168.1 1.6 copy.16

commit v3 on v2

--- a/solution.py
+++ b/solution.py
@@ -17,8 +17,8 @@
     return lax.dot_general(a, b, (((0,), (0,)), ((), ())), preferred_element_type=jnp.float32)
 
 
-def kernel(x_ref, d_ref, wg_ref, wu_ref, wd_ref, gi, og, ou, od, xo0, xo1, do0, do1, xp, dp, rx, rd, xs, ds, fx, fd, wv, xv, dv, back_ref, hv, h1, hp0, hp1, dxv, r1, r2, r3, t1, t2, t3, wr, send, recv, local):
-    xo, do = (xo0, xo1), (do0, do1)
+def kernel(x_ref, d_ref, wg_ref, wu_ref, wd_ref, gi, og, ou, od, xo0, xo1, do0, do1, xp, dp, xs, ds, fx, fd, wv, xv, dv, back_ref, hv, h1, hp0, hp1, dxv, r1, r2, r3, t1, t2, t3, wr, send, recv, local):
+    xo, do = (xv, xo1), (dv, do1)
     rep, fs, tp = lax.axis_index("rep"), lax.axis_index("fs"), lax.axis_index("tp")
     core = fs % 2
     xc = rep * 2 + fs // 2
@@ -27,7 +27,7 @@
     def at_x(v):
         return {"rep": v // 2, "fs": (v % 2) * 2 + core}
 
-    xright, xleft, xfar = at_x((xc + 1) % 4), at_x((xc + 3) % 4), {"rep": 1 - rep}
+    xright, xleft = at_x((xc + 1) % 4), at_x((xc + 3) % 4)
     yright, yleft = {"tp": z * 4 + (y + 1) % 4}, {"tp": z * 4 + (y + 3) % 4}
     zright, zleft = {"tp": ((z + 1) % 4) * 4 + y}, {"tp": ((z + 3) % 4) * 4 + y}
     partner = {"fs": fs + 1 - 2 * core}
@@ -60,9 +60,9 @@
         ready.append(keep(ref, wv.at[m, :, block(0)]))
 
     barrier = pltpu.get_barrier_semaphore()
-    for dev in (xright, xleft, xfar, yright, yleft, zright, zleft, partner):
+    for dev in (xright, xleft, yright, yleft, zright, zleft, partner):
         pl.semaphore_signal(barrier, inc=1, device_id=dev, device_id_type=MESH)
-    pl.semaphore_wait(barrier, 8)
+    pl.semaphore_wait(barrier, 7)
     for copy in ready[:8]:
         copy.wait()
 
@@ -108,7 +108,7 @@
         return x, d
 
     def second_axis_far(k, c):
-        first, second = ((pl.ds(0, 2), pl.ds(2, 2)), (pl.ds(0, 1), pl.ds(3, 1)))[k]
+        first, second = ((pl.ds(0, 2), pl.ds(2, 2)), (pl.ds(0, 2), pl.ds(2, 2)))[k]
         x, d = c
         x[0].wait_recv()
         a = put(xo[k].at[1, first], xo[k].at[3, first], zright)
@@ -154,12 +154,12 @@
         put(wv.at[1, tail, block(0)], wv.at[1, tail, block(1)], xleft),
     ]
     own2 = first_axis_far(0, own1)
+    for copy in own0:
+        copy.wait()
+    own3 = second_axis(0, own2)
     far[0].wait_recv()
     far[1].wait_recv()
     far1 = first_axis(1, xo[1].at[0, 0], do[1].at[0, 0])
-    for copy in own0:
-        copy.wait()
-    own3 = second_axis(0, own2)
     far2 = first_axis_far(1, far1)
     own4 = second_axis_far(0, own3)
     w2[0].wait_recv()
@@ -172,14 +172,12 @@
     w2[3].wait_recv()
     w3.append(put(wv.at[1, :, block(1)], wv.at[1, :, block(3)], partner))
     finish(0, own4)
-    middle = pl.ds(1, 2)
-    helped = [put(xo0.at[3, middle], rx, xright), put(do0.at[middle, 3], rd, xleft)]
-
-    whole = [keep(xo0, xv), keep(do0, dv)]
+
+    early = len(started)
+    sent = list(started)
+    whole = [keep(xv, xo0), keep(dv, do0)]
     for copy in w1 + w3:
         copy.wait_recv()
-    for copy in whole:
-        copy.wait()
 
     def forward(ref, m, acts, n):
         rows = acts[pl.ds(n * 2, 2)].reshape(256, 4096)
@@ -205,14 +203,14 @@
         def _(n):
             forward((hv.at[0], hv.at[1], back_ref)[m], m, acts, n)
 
-    helped[0].wait_recv()
-    relay = [put(rx, xo1.at[3, middle], xright)]
-    helped[1].wait_recv()
-    relay.append(put(rd, do1.at[middle, 3], xleft))
     far4 = second_axis_far(1, far3)
     pointwise(hv, True, True)
     swap0 = put(hv, hp0, partner)
     rest(1, far3)
+    for copy in whole:
+        copy.wait()
+    for copy in sent:
+        copy.wait_send()
     whole = [keep(xo1.at[first], xv.at[first]), keep(xo1.at[2], xv.at[2]), keep(do1.at[:, pl.ds(0, 3)], dv.at[:, pl.ds(0, 3)])]
 
     @pl.loop(0, 8)
@@ -250,8 +248,6 @@
     whole[0].wait()
     forward(h1.at[0], 0, xv, 0)
     forward(h1.at[1], 1, xv, 0)
-    for copy in relay:
-        copy.wait_recv()
     finish(1, far4)
     last_x, last_d = keep(xo1.at[3], xv.at[3]), keep(do1.at[:, 3], dv.at[:, 3])
     whole[1].wait()
@@ -269,7 +265,7 @@
             for q, source in enumerate((tokens[0].at[:, :, :, block(r)], tokens[1].at[:, :, :, block(r)], theirs.at[0, :, :, :, block(r)], theirs.at[1, :, :, :, block(r)]))
         ]
 
-    loads_x = load(0, xo, xp, 1)
+    loads_x = load(0, (xo0, xo1), xp, 1)
     whole[2].wait()
     last_d.wait()
 
@@ -277,7 +273,7 @@
     def _(n):
         forward(back_ref, 2, dv, n)
 
-    loads_d = load(1, do, dp, 1)
+    loads_d = load(1, (do0, do1), dp, 1)
     pointwise(h1, False, True)
     for m in range(2):
         swaps[m] = put(h1.at[m], hp1.at[m], partner)
@@ -320,10 +316,8 @@
         copy.wait()
     swap0.wait_recv()
     swaps[2].wait_recv()
-    for copy in w1 + w2:
-        copy.wait_send()
     outgoing(2, dv)
-    loads_d = load(1, do, dp, 0)
+    loads_d = load(1, (do0, do1), dp, 0)
     sums2 = [send_summed(slab, ways[c], c, r1, r2, sums1[c]) for c in range(2)]
     for copy in loads_x:
         copy.wait()
@@ -331,7 +325,7 @@
     outgoing(0, xv)
     swaps[1].wait_recv()
     outgoing(1, xv)
-    loads_x = load(0, xo, xp, 0)
+    loads_x = load(0, (xo0, xo1), xp, 0)
     sums3 = []
     for c in range(2):
         sums1[c][3].wait_recv()
@@ -360,9 +354,8 @@
             gi[:, pl.ds(pl.multiple_of(owners[2 * c + h] * 1024, 1024), 1024)] = total.astype(jnp.bfloat16)
     close(0, og)
     close(1, ou)
-    for copy in started:
-        if not any(copy is done for done in w1 + w2):
-            copy.wait_send()
+    for copy in started[early:]:
+        copy.wait_send()
 
 
 SENDS, KEPT, LIMIT = 120, 42, 58000000
@@ -375,9 +368,9 @@
     s = jax.ShapeDtypeStruct
     outs = pl.pallas_call(
         kernel,
-        out_shape=[pltpu.VMEM((32, 4096), b)] + [pltpu.VMEM((688, 1024), f)] * 3 + [s((4, 4, 32, 4096), b)] * 4 + [s((2, 4, 4, 32, 2048), b)] * 2 + [s((2, 32, 4096), b)] * 2,
+        out_shape=[pltpu.VMEM((32, 4096), b)] + [pltpu.VMEM((688, 1024), f)] * 3 + [s((4, 4, 32, 4096), b)] * 4 + [s((2, 4, 4, 32, 2048), b)] * 2,
         in_specs=[anys] * 5,
-        out_specs=[vm] * 4 + [anys] * 8,
+        out_specs=[vm] * 4 + [anys] * 6,
         scratch_shapes=[pltpu.VMEM((32, 4096), b)] * 4
         + [pltpu.VMEM((3, 688, 4096), b)]
         + [pltpu.VMEM((4, 4, 32, 4096), b)] * 2

time: 170 us -> 166 us (0.976)
  Pallas kernels: 164 us -> 160 us
    pallas_call x1, Pallas kernels: 164 us -> 160 us  [body(): pl.pallas_call(kernel, out_shape=[pltpu.VMEM((32, 4096), b)] + [pltpu.VME...]
where the time goes in v3:
time: 166 us
  Pallas kernels  160 us (96%)
  local copies, waits for them, and re-layouts  5.37 us (3%)
    pallas_call x1, Pallas kernels, body(): pl.pallas_call(kernel, out_shape=[pltpu.VMEM((32, 4096), b)] + [pltpu.VME...  160 us
    unnamed x4, local copies, waits for them, and re-layouts  5.37 us

profile of v3, /device:TPU:0, one launch (start us, length us, event | category | flops | bytes accessed | tf_op | source)
XLA Modules:
  0.0 166.4 jit_solution(9133700187316824177)
XLA Ops:
  0.6 160.3 %shard_map.84 = (bf16[32,4096]{1,0:T(8,128)(2,1)S(1)}, f32[688,1024]{1,0:T(8,128)S(1)}, f32[688,1024]{1,0:T(8,128)S(1)}, f32[688,1024]{1,0:T(8,128)S(1)}, bf16[4...) custom-call(bf16[32,4096]{1,0:T(8,128)(2,1)} %x_ref.1, ...), custom_call_target="tpu_custom_call" | custom-call | tf_op jit(solution)/shard_map/pallas_call | solution.py:369
  161.0 0.7 copy.13
  161.7 1.6 copy.14
  163.2 1.6 copy.15
  164.8 1.6 copy.16

commit v4 on v3

--- a/solution.py
+++ b/solution.py
@@ -289,12 +289,12 @@
     crossing = {}
 
     def outgoing(m, acts):
-        for half in range(2):
-            @pl.loop(2 * half, 2 * half + 2)
+        for half in range(4):
+            @pl.loop(half, half + 1)
             def _(n):
                 wv[m, :, pl.ds(pl.multiple_of(n * 256, 256), 256)] = product(m, acts, n).astype(jnp.bfloat16)
 
-            span = pl.ds(512 * half, 512)
+            span = pl.ds(256 * half, 256)
             crossing[m, half] = [put(wv.at[m, head, span], wr.at[m, head, span], xright), put(wv.at[m, tail, span], wr.at[m, tail, span], xleft)]
 
     def kept(m, acts, ref):
@@ -303,11 +303,11 @@
             ref[:, pl.ds(pl.multiple_of(n * 256, 256), 256)] = product(m, acts, n)
 
     def close(m, ref):
-        for half in range(2):
+        for half in range(4):
             for copy in crossing[m, half]:
                 copy.wait_recv()
 
-            @pl.loop(2 * half, 2 * half + 2)
+            @pl.loop(half, half + 1)
             def _(n):
                 span = pl.ds(pl.multiple_of(n * 256, 256), 256)
                 ref[:, span] += wr[m, :, span].astype(jnp.float32)
@@ -326,6 +326,9 @@
     swaps[1].wait_recv()
     outgoing(1, xv)
     loads_x = load(0, (xo0, xo1), xp, 0)
+    for copy in loads_d:
+        copy.wait()
+    kept(2, dv, od)
     sums3 = []
     for c in range(2):
         sums1[c][3].wait_recv()
@@ -335,14 +338,11 @@
         sums2[c][1].wait_recv()
         r2[c, 1] += slab(c, 0, 1)[...] + r3[c, 1]
         sums3.append(send_raw(part, ways[1 - c], c, t1, t3))
-    for copy in loads_d:
-        copy.wait()
-    kept(2, dv, od)
     for copy in loads_x:
         copy.wait()
     kept(0, xv, og)
+    sums4 = [send_summed(part, ways[1 - c], c, t1, t2, sums3[c]) for c in range(2)]
     kept(1, xv, ou)
-    sums4 = [send_summed(part, ways[1 - c], c, t1, t2, sums3[c]) for c in range(2)]
     close(2, od)
     for c in range(2):
         sums3[c][3].wait_recv()
@@ -358,7 +358,7 @@
         copy.wait_send()
 
 
-SENDS, KEPT, LIMIT = 120, 42, 58000000
+SENDS, KEPT, LIMIT = 132, 42, 58000000
 
 
 def body(inputs, w_gate, w_up, w_down, d_out):

time: 166 us -> 166 us (level)
  no operation moved by 1% of the time
where the time goes in v4:
time: 166 us
  Pallas kernels  160 us (96%)
  local copies, waits for them, and re-layouts  5.37 us (3%)
    pallas_call x1, Pallas kernels, body(): pl.pallas_call(kernel, out_shape=[pltpu.VMEM((32, 4096), b)] + [pltpu.VME...  160 us
    unnamed x4, local copies, waits for them, and re-layouts  5.37 us

profile of v4, /device:TPU:0, one launch (start us, length us, event | category | flops | bytes accessed | tf_op | source)
XLA Modules:
  0.0 166.3 jit_solution(7303893514518433512)
XLA Ops:
  0.6 160.2 %shard_map.84 = (bf16[32,4096]{1,0:T(8,128)(2,1)S(1)}, f32[688,1024]{1,0:T(8,128)S(1)}, f32[688,1024]{1,0:T(8,128)S(1)}, f32[688,1024]{1,0:T(8,128)S(1)}, bf16[4...) custom-call(bf16[32,4096]{1,0:T(8,128)(2,1)} %x_ref.1, ...), custom_call_target="tpu_custom_call" | custom-call | tf_op jit(solution)/shard_map/pallas_call | solution.py:369
  160.9 0.7 copy.13
  161.6 1.6 copy.14
  163.1 1.6 copy.15
  164.7 1.6 copy.16

commit v5 on v4

--- a/solution.py
+++ b/solution.py
@@ -256,8 +256,6 @@
     forward(h1.at[1], 1, xv, 1)
     pointwise(h1, True, False)
     swaps = {2: put(h1.at[2], hp1.at[2], partner)}
-    for copy in gathered:
-        copy.wait_recv()
 
     def load(k, tokens, theirs, r):
         return [
@@ -265,7 +263,6 @@
             for q, source in enumerate((tokens[0].at[:, :, :, block(r)], tokens[1].at[:, :, :, block(r)], theirs.at[0, :, :, :, block(r)], theirs.at[1, :, :, :, block(r)]))
         ]
 
-    loads_x = load(0, (xo0, xo1), xp, 1)
     whole[2].wait()
     last_d.wait()
 
@@ -273,7 +270,10 @@
     def _(n):
         forward(back_ref, 2, dv, n)
 
+    for copy in gathered:
+        copy.wait_recv()
     loads_d = load(1, (do0, do1), dp, 1)
+    loads_x = load(0, (xo0, xo1), xp, 1)
     pointwise(h1, False, True)
     for m in range(2):
         swaps[m] = put(h1.at[m], hp1.at[m], partner)

time: 166 us -> 166 us (level)
  no operation moved by 1% of the time
where the time goes in v5:
time: 166 us
  Pallas kernels  160 us (96%)
  local copies, waits for them, and re-layouts  5.37 us (3%)
    pallas_call x1, Pallas kernels, body(): pl.pallas_call(kernel, out_shape=[pltpu.VMEM((32, 4096), b)] + [pltpu.VME...  160 us
    unnamed x4, local copies, waits for them, and re-layouts  5.37 us

profile of v5, /device:TPU:0, one launch (start us, length us, event | category | flops | bytes accessed | tf_op | source)
XLA Modules:
  0.0 165.7 jit_solution(2201022875374990455)
XLA Ops:
  0.6 159.7 %shard_map.84 = (bf16[32,4096]{1,0:T(8,128)(2,1)S(1)}, f32[688,1024]{1,0:T(8,128)S(1)}, f32[688,1024]{1,0:T(8,128)S(1)}, f32[688,1024]{1,0:T(8,128)S(1)}, bf16[4...) custom-call(bf16[32,4096]{1,0:T(8,128)(2,1)} %x_ref.1, ...), custom_call_target="tpu_custom_call" | custom-call | tf_op jit(solution)/shard_map/pallas_call | solution.py:369
  160.4 0.7 copy.13
  161.1 1.6 copy.14
  162.6 1.6 copy.15
  164.2 1.6 copy.16
